TPU v7x, 32 devices: a whole 2x2x4 slice. The times are simulated.
32 devices in a mesh: fs: 16 (over z, y, x), tp: 2 (over core).
Axes of the slice: x: 2, y: 2, z: 4, core: 2. Of those that a mesh axis runs over, the one named last changes fastest.
Arguments:
- tokens: bfloat16 [8192, 2048], P('fs', 'tp'), may hold values from -6 to 6
- norm_gain: bfloat16 [2048], P('tp'), may hold values from 0.099609375 to 1.8984375
- proj_u: bfloat16 [2048, 2048], P('fs', 'tp'), may hold values from -0.125 to 0.125
- proj_v: bfloat16 [2048, 2048], P('fs', 'tp'), may hold values from -0.125 to 0.125
- layer_gain: bfloat16 [2048], P('tp'), may hold values from 0.099609375 to 1.8984375
- layer_shift: bfloat16 [2048], P('tp'), may hold values from -3 to 3
- mix_weight: bfloat16 [16, 128, 128], P('tp'), may hold values from -0.5 to 0.5
- mix_bias: bfloat16 [16, 128], P('tp'), may hold values from 0.099609375 to 1.8984375
- proj_out: bfloat16 [2048, 2048], P('tp', 'fs'), may hold values from -0.1875 to 0.1875
- ffn_gain: bfloat16 [2048], P('tp'), may hold values from 0.099609375 to 1.8984375
- ffn_gate: bfloat16 [2048, 4096], P('fs', 'tp'), may hold values from -0.125 to 0.125
- ffn_value: bfloat16 [2048, 4096], P('fs', 'tp'), may hold values from -0.125 to 0.125
- conv_gate: bfloat16 [3, 4096], P(None, 'tp'), may hold values from -3 to 3
- conv_value: bfloat16 [3, 4096], P(None, 'tp'), may hold values from -3 to 3
- proj_down: bfloat16 [4096, 2048], P('tp', 'fs'), may hold values from -0.125 to 0.125
Outputs:
- result: bfloat16 [8192, 2048], P('fs', 'tp')
All inputs are finite; a program needn't handle non-finite values.
Results may differ from a plain program's by a relative error of at most 0.017.
Values may be sent and summed in bfloat16 or wider, within the bound.
A program may use at most 64 MiB of HBM per device.

v0:
```python
import jax
import jax.numpy as jnp
from jax import lax
from jax.sharding import PartitionSpec as P

GROUP_DIM = 128
BLOCK = 128
SEGMENT = 64
KERNEL = 3
SEQ_LEN = 256
EPS = 1e-06


def matmul(operand, matrix):
    return jnp.dot(operand, matrix, preferred_element_type=jnp.float32)


def local_rms(values_in, gain_row):
    values = values_in.astype(jnp.float32)
    scale_row = lax.rsqrt(jnp.mean(values * values, axis=1, keepdims=True) + EPS)
    return (values * scale_row * gain_row.astype(jnp.float32)).astype(jnp.bfloat16)


def causal_taps(values, weights):
    seq_count = values.shape[0] // SEQ_LEN
    shaped = values.reshape(seq_count, SEQ_LEN, values.shape[1])
    padded = jnp.pad(shaped, ((0, 0), (KERNEL - 1, 0), (0, 0)))
    summed = jnp.zeros(shaped.shape, jnp.float32)
    for tap_index in range(KERNEL):
        summed = summed + padded[:, tap_index : tap_index + SEQ_LEN].astype(jnp.float32) * weights[
            tap_index
        ].astype(jnp.float32)
    return summed.reshape(values.shape[0], values.shape[1])


def on_device(
    tokens,
    norm_gain,
    proj_u,
    proj_v,
    layer_gain,
    layer_shift,
    mix_weight,
    mix_bias,
    proj_out,
    ffn_gain,
    ffn_gate,
    ffn_value,
    conv_gate,
    conv_value,
    proj_down,
):
    own_width = tokens.shape[1]
    whole_tokens, whole_gain, whole_ffn_gain = (
        lax.all_gather(tokens, "tp", axis=1, tiled=True),
        lax.all_gather(norm_gain, "tp", axis=0, tiled=True),
        lax.all_gather(ffn_gain, "tp", axis=0, tiled=True),
    )
    normed = local_rms(whole_tokens, whole_gain)
    row_count = normed.shape[0]
    whole_u, whole_v = (
        lax.all_gather(proj_u, "fs", axis=0, tiled=True),
        lax.all_gather(proj_v, "fs", axis=0, tiled=True),
    )
    pre_u = matmul(normed, whole_u)
    pre_v = matmul(normed, whole_v)
    act_u = jax.nn.gelu(pre_u, approximate=False)
    act_v = jax.nn.gelu(pre_v, approximate=False)
    full_width = act_v.shape[1] * lax.axis_size("tp")
    total_sum, second = lax.psum((jnp.sum(act_v, axis=1), jnp.sum(act_v * act_v, axis=1)), "tp")
    center = total_sum / full_width
    spread = second / full_width - center * center
    mixed_in = (
        (act_v - center[:, None])
        * lax.rsqrt(spread + EPS)[:, None]
        * layer_gain.astype(jnp.float32)
        + layer_shift.astype(jnp.float32)
    ).astype(jnp.bfloat16)
    groups = mixed_in.shape[1] // GROUP_DIM
    blocks = mixed_in.reshape(row_count // BLOCK, BLOCK, groups, GROUP_DIM)
    segment = jnp.arange(BLOCK) // SEGMENT
    visible = segment[None, :] <= segment[:, None]
    masked = jnp.where(visible[None], mix_weight, jnp.zeros_like(mix_weight))
    spatial = (
        jnp.einsum("gij,njgc->nigc", masked, blocks, preferred_element_type=jnp.float32)
        + mix_bias.astype(jnp.float32).T[None, :, :, None]
    )
    gated_rows = (act_u * spatial.reshape(row_count, mixed_in.shape[1])).astype(jnp.bfloat16)
    whole_out = lax.all_gather(proj_out, "fs", axis=1, tiled=True)
    partial_value = matmul(gated_rows, whole_out)
    summed = lax.psum(partial_value.astype(jnp.bfloat16), "tp").astype(jnp.float32)
    stream_rows = (whole_tokens.astype(jnp.float32) + summed).astype(jnp.bfloat16)
    normed_two = local_rms(stream_rows, whole_ffn_gain)
    stream = lax.dynamic_slice_in_dim(stream_rows, lax.axis_index("tp") * own_width, own_width, 1)
    whole_gate, whole_value = (
        lax.all_gather(ffn_gate, "fs", axis=0, tiled=True),
        lax.all_gather(ffn_value, "fs", axis=0, tiled=True),
    )
    pre_gate = matmul(normed_two, whole_gate)
    pre_value = matmul(normed_two, whole_value)
    conv_g = causal_taps(pre_gate.astype(jnp.bfloat16), conv_gate)
    conv_v = causal_taps(pre_value.astype(jnp.bfloat16), conv_value)
    hidden = (jax.nn.silu(conv_g) * conv_v).astype(jnp.bfloat16)
    whole_down = lax.all_gather(proj_down, "fs", axis=1, tiled=True)
    partial_two = matmul(hidden, whole_down)
    return (
        stream.astype(jnp.float32)
        + lax.psum_scatter(
            partial_two.astype(jnp.bfloat16), "tp", scatter_dimension=1, tiled=True
        ).astype(jnp.float32)
    ).astype(jnp.bfloat16)


def solution(mesh):
    in_specs = (
        P("fs", "tp"),
        P("tp"),
        P("fs", "tp"),
        P("fs", "tp"),
        P("tp"),
        P("tp"),
        P("tp", None, None),
        P("tp", None),
        P("tp", "fs"),
        P("tp"),
        P("fs", "tp"),
        P("fs", "tp"),
        P(None, "tp"),
        P(None, "tp"),
        P("tp", "fs"),
    )
    out_specs = P("fs", "tp")
    return jax.shard_map(
        on_device, mesh=mesh, in_specs=in_specs, out_specs=out_specs, check_vma=False
    )
```

profile of v0, /device:TPU:0, one launch (start us, length us, event | category | flops | bytes accessed | tf_op | source)
XLA Modules:
  0.0 702.0 jit_solution(10624210363305999877)
XLA Ops:
  6.5 0.7 all-gather.8.cloned.1.call-update
  7.3 0.0 all-gather.12.cloned.1.call-start
  7.3 0.7 all-gather.12.cloned.1.call-update
  8.0 0.0 all-gather.10.cloned.1.call-start
  8.1 0.7 all-gather.10.cloned.1.call-update
  8.7 0.0 all-gather.14.cloned.1.call-start
  8.8 0.5 all-gather.14.cloned.1.call-update
  9.3 0.0 all-reduce.5.cloned.1.call-start
  9.4 2.1 all_gather.28
  11.5 0.7 convert_element_type.146
  12.2 0.7 convert_element_type.147
  12.9 0.7 convert_bitcast_fusion
  13.5 0.1 broadcast_compare_fusion
  13.6 8.6 %all-gather.8.cloned.1.call-done = bf16[512,2048]{1,0:T(8,128)(2,1)} async-done(((bf16[512,1024]{1,0:T(8,128)(2,1)}), bf16[512,2048]{1,0:T(8,128)(2,1)}) %all-gather.8.cloned.1.call-update) | async-done | bytes 2097168 | tf_op jit(solution)/shard_map/all_gather | solution.py:55
  22.2 2.2 fusion.3
  24.4 77.3 %all-gather.12.cloned.1.call-done = bf16[2048,1024]{1,0:T(8,128)(2,1)} async-done(((bf16[128,1024]{1,0:T(8,128)(2,1)}), bf16[2048,1024]{1,0:T(8,128)(2,1)}) %all-gather.12.cloned.1.call-update) | async-done | bytes 4194320 | tf_op jit(solution)/shard_map/all_gather | solution.py:63
  101.8 9.6 %fusion.111 = (f32[512]{0:T(512)S(1)}, f32[512]{0:T(512)S(1)}, f32[512,1024]{1,0:T(8,128)}) fusion(bf16[2048,1024]{1,0:T(8,128)(2,1)} %all-gather.12.cloned.1.call-done, bf16[512,2048]{1,0:T(8,128)(2,1)S(1)} %copy-done, f32[2048]{0:T(1024)S(1)} %convert_element_type.144, f32[512]{0:T(512)S(1)} %add_rsqrt_fusion.2), kind=kOutput, calls=%fused_computation.152 | convolution fusion | flops 2186804224 | bytes 8402944 | tf_op jit(solution)/shard_map/dot_general | solution.py:15
  111.4 2.6 all-reduce.2
  114.1 2.1 fusion.32
  116.2 0.3 copy.21
  116.4 1.9 bitcast_add_fusion
  118.3 2.9 copy.19
  121.2 57.5 %all-gather.10.cloned.1.call-done = bf16[2048,1024]{1,0:T(8,128)(2,1)} async-done(((bf16[128,1024]{1,0:T(8,128)(2,1)}), bf16[2048,1024]{1,0:T(8,128)(2,1)}) %all-gather.10.cloned.1.call-update) | async-done | bytes 4194320 | tf_op jit(solution)/shard_map/all_gather | solution.py:62
  178.8 89.9 %all-gather.14.cloned.1.call-done = bf16[1024,2048]{1,0:T(8,128)(2,1)} async-done(((bf16[1024,128]{1,0:T(8,128)(2,1)}), bf16[1024,2048]{1,0:T(8,128)(2,1)}) %all-gather.14.cloned.1.call-update) | async-done | bytes 4194320 | tf_op jit(solution)/shard_map/all_gather | solution.py:89
  268.7 14.5 %convolution_convert_fusion = bf16[512,2048]{1,0:T(8,128)(2,1)} fusion(bf16[1024,2048]{1,0:T(8,128)(2,1)} %all-gather.14.cloned.1.call-done, f32[64,8,8,128]{3,2,1,0:T(8,128)} %bitcast.51, bf16[2048,1024]{1,0:T(8,128)(2,1)} %all-gather.10.cloned.1.call-done, bf16[512,2048]{1,0:T(8,128)(2,1)S(1)} %copy-done, f32[2048]{0:T(1024)S(1)} %convert_element_type.144, ...), kind=kOutput, calls=%fused_computation.23 | convolution fusion | flops 4334813184 | bytes 14690304 | tf_op jit(solution)/shard_map/dot_general | solution.py:15
  283.2 0.0 all-reduce.5.cloned.1.call-update
  283.2 0.0 all-gather.16.cloned.1.call-start
  283.3 0.5 all-gather.16.cloned.1.call-update
  283.8 0.0 all-gather.18.cloned.1.call-start
  283.8 0.7 all-gather.18.cloned.1.call-update
  284.5 0.0 all-gather.20.cloned.1.call-start
  284.6 0.7 all-gather.20.cloned.1.call-update
  285.3 0.0 reduce-scatter.2.cloned.1.call-start
  285.3 2.1 all_gather.32
  287.5 15.4 %all-reduce.5.cloned.1.call-done = bf16[512,2048]{1,0:T(8,128)(2,1)} async-done(((bf16[512,2048]{1,0:T(8,128)(2,1)}), bf16[512,2048]{1,0:T(8,128)(2,1)}) %all-reduce.5.cloned.1.call-update) | async-done | bytes 2097168 | tf_op jit(solution)/shard_map/psum | solution.py:91
  302.8 3.9 fusion
  306.8 112.2 %all-gather.16.cloned.1.call-done = bf16[2048,2048]{1,0:T(8,128)(2,1)} async-done(((bf16[128,2048]{1,0:T(8,128)(2,1)}), bf16[2048,2048]{1,0:T(8,128)(2,1)}) %all-gather.16.cloned.1.call-update) | async-done | bytes 8388624 | tf_op jit(solution)/shard_map/all_gather | solution.py:96
  419.0 10.0 %convolution_convert_fusion.3 = bf16[512,2048]{1,0:T(8,128)(2,1)} fusion(bf16[2048,2048]{1,0:T(8,128)(2,1)} %all-gather.16.cloned.1.call-done, bf16[512,2048]{1,0:T(8,128)(2,1)} %get-tuple-element.10, f32[2048]{0:T(1024)S(1)} %convert_element_type.155, f32[512]{0:T(512)S(1)} %add_rsqrt_fusion), kind=kOutput, calls=%fused_computation.26 | convolution fusion | flops 4300210176 | bytes 12593152 | tf_op jit(solution)/shard_map/dot_general | solution.py:15
  429.0 103.2 %all-gather.18.cloned.1.call-done = bf16[2048,2048]{1,0:T(8,128)(2,1)} async-done(((bf16[128,2048]{1,0:T(8,128)(2,1)}), bf16[2048,2048]{1,0:T(8,128)(2,1)}) %all-gather.18.cloned.1.call-update) | async-done | bytes 8388624 | tf_op jit(solution)/shard_map/all_gather | solution.py:97
  532.2 8.4 %convolution_convert_fusion.2 = bf16[512,2048]{1,0:T(8,128)(2,1)S(1)} fusion(bf16[2048,2048]{1,0:T(8,128)(2,1)} %all-gather.18.cloned.1.call-done, bf16[512,2048]{1,0:T(8,128)(2,1)S(1)} %copy-done.1, f32[2048]{0:T(1024)S(1)} %convert_element_type.155, f32[512]{0:T(512)S(1)} %add_rsqrt_fusion), kind=kOutput, calls=%fused_computation.25 | convolution fusion | flops 4300210176 | bytes 12593152 | tf_op jit(solution)/shard_map/dot_general | solution.py:15
  540.6 0.0 copy-done.2
  540.7 3.0 multiply_add_fusion
  543.7 2.6 fusion.7
  546.3 128.7 %all-gather.20.cloned.1.call-done = bf16[2048,2048]{1,0:T(8,128)(2,1)} async-done(((bf16[2048,128]{1,0:T(8,128)(2,1)}), bf16[2048,2048]{1,0:T(8,128)(2,1)}) %all-gather.20.cloned.1.call-update) | async-done | bytes 8388624 | tf_op jit(solution)/shard_map/all_gather | solution.py:104
  675.0 9.9 %convolution_convert_fusion.1 = bf16[512,2048]{1,0:T(8,128)(2,1)} fusion(bf16[512,2048]{1,0:T(8,128)(2,1)} %fusion.7, bf16[2048,2048]{1,0:T(8,128)(2,1)} %all-gather.20.cloned.1.call-done), kind=kOutput, calls=%fused_computation.24 | convolution fusion | flops 4296015872 | bytes 12582912 | tf_op jit(solution)/shard_map/dot_general | solution.py:15
  684.9 0.0 reduce-scatter.2.cloned.1.call-update
  684.9 8.0 %reduce-scatter.2.cloned.1.call-done = bf16[512,1024]{1,0:T(8,128)(2,1)} async-done(((bf16[512,2048]{1,0:T(8,128)(2,1)}), bf16[512,1024]{1,0:T(8,128)(2,1)}) %reduce-scatter.2.cloned.1.call-update) | async-done | bytes 1048592 | tf_op jit(solution)/shard_map/reduce_scatter | solution.py:108
  692.9 2.6 add_convert_fusion
  (22 shorter events, 0.1 us)
Async XLA Ops:
  6.5 15.7 %all-gather.8.cloned.1.call-start = ((), (), s32[]{:S(2)}) async-start(), calls=%async_computation.1 | async-start | bytes 3145728 | tf_op jit(solution)/shard_map/all_gather | solution.py:55
  7.3 94.5 %all-gather.12.cloned.1.call-start = ((), (), s32[]{:S(2)}) async-start(), calls=%async_computation.3 | async-start | bytes 4456448 | tf_op jit(solution)/shard_map/all_gather | solution.py:63
  8.0 170.8 %all-gather.10.cloned.1.call-start = ((), (), s32[]{:S(2)}) async-start(), calls=%async_computation.2 | async-start | bytes 4456448 | tf_op jit(solution)/shard_map/all_gather | solution.py:62
  8.7 259.9 %all-gather.14.cloned.1.call-start = ((), (), s32[]{:S(2)}) async-start(), calls=%async_computation.4 | async-start | bytes 4456448 | tf_op jit(solution)/shard_map/all_gather | solution.py:89
  9.3 293.5 %all-reduce.5.cloned.1.call-start = ((), (), s32[]{:S(2)}) async-start(), calls=%async_computation.5 | async-start | bytes 4194304 | tf_op jit(solution)/shard_map/psum | solution.py:91
  22.2 79.6 %copy-start = (bf16[512,2048]{1,0:T(8,128)(2,1)S(1)}, bf16[512,2048]{1,0:T(8,128)(2,1)}, u32[]{:S(2)}) copy-start(bf16[512,2048]{1,0:T(8,128)(2,1)} %all-gather.8.cloned.1.call-done) | copy-start | bytes 6291460
  114.1 2.4 copy-start.3
  283.2 2.2 copy-start.6
  283.2 4.2 copy-start.4
  283.2 4.3 copy-start.5
  283.2 135.8 %all-gather.16.cloned.1.call-start = ((), (), s32[]{:S(2)}) async-start(), calls=%async_computation.6 | async-start | bytes 8912896 | tf_op jit(solution)/shard_map/all_gather | solution.py:96
  283.8 248.4 %all-gather.18.cloned.1.call-start = ((), (), s32[]{:S(2)}) async-start(), calls=%async_computation.7 | async-start | bytes 8912896 | tf_op jit(solution)/shard_map/all_gather | solution.py:97
  284.5 390.4 %all-gather.20.cloned.1.call-start = ((), (), s32[]{:S(2)}) async-start(), calls=%async_computation.8 | async-start | bytes 8912896 | tf_op jit(solution)/shard_map/all_gather | solution.py:104
  285.3 407.6 %reduce-scatter.2.cloned.1.call-start = ((), (), s32[]{:S(2)}) async-start(), calls=%async_computation.9 | async-start | bytes 3145728 | tf_op jit(solution)/shard_map/reduce_scatter | solution.py:108
  419.0 113.3 %copy-start.1 = (bf16[512,2048]{1,0:T(8,128)(2,1)S(1)}, bf16[512,2048]{1,0:T(8,128)(2,1)}, u32[]{:S(2)}) copy-start(bf16[512,2048]{1,0:T(8,128)(2,1)} %get-tuple-element.10) | copy-start | bytes 6291460
  532.2 8.4 %copy-start.2 = (bf16[512,2048]{1,0:T(8,128)(2,1)S(1)}, bf16[512,2048]{1,0:T(8,128)(2,1)}, u32[]{:S(2)}) copy-start(bf16[512,2048]{1,0:T(8,128)(2,1)} %convolution_convert_fusion.3) | copy-start | bytes 6291460
Sparse Core Ops, SparseCore 0:
  8.9 13.2 all-gather.7
  25.0 76.7 all-gather.11
  104.5 74.1 all-gather.9
  181.3 87.3 all-gather.13
  283.3 19.4 all-reduce.4
  305.5 113.4 all-gather.15
  421.7 110.4 all-gather.17
  534.9 139.9 all-gather.19
  685.0 7.7 reduce-scatter.1
where the time goes:
time: 702 us
  waiting for transfers between devices  605 us (86%)
  matrix products  54.3 us (8%)
  other arithmetic  18.7 us (3%)
  between operations  13.3 us (2%)
    all_gather x1, waiting for transfers between devices, on_device(): whole_down = lax.all_gather(proj_down, 'fs', axis=1, tiled=True)  129 us
    all_gather x1, waiting for transfers between devices, on_device(): lax.all_gather(ffn_gate, 'fs', axis=0, tiled=True)  112 us
    all_gather x1, waiting for transfers between devices, on_device(): lax.all_gather(ffn_value, 'fs', axis=0, tiled=True)  103 us
    all_gather x1, waiting for transfers between devices, on_device(): whole_out = lax.all_gather(proj_out, 'fs', axis=1, tiled=True)  89.9 us
    all_gather x1, waiting for transfers between devices, on_device(): lax.all_gather(proj_v, 'fs', axis=0, tiled=True)  77.3 us
    all_gather x1, waiting for transfers between devices, on_device(): lax.all_gather(proj_u, 'fs', axis=0, tiled=True)  57.5 us
    dot_general x5, matrix products, matmul(): return jnp.dot(operand, matrix, preferred_element_type=jnp.float32)  52.5 us
    psum x1, waiting for transfers between devices, on_device(): lax.psum(partial_value.astype(jnp.bfloat16), 'tp').astype(jnp.float32)  15.4 us
  transfers between devices with their start and end apart: 9, of which 9 were waited for; matrix products, arithmetic and copies ran while one was open for 7% of the time, Pallas kernels for 0%

commit v1 on v0

--- a/solution.py
+++ b/solution.py
@@ -2,6 +2,7 @@
 import jax.numpy as jnp
 from jax import lax
 from jax.sharding import PartitionSpec as P
+from jax.lax import axis_index, axis_size, ppermute
 
 GROUP_DIM = 128
 BLOCK = 128
@@ -9,6 +10,19 @@
 KERNEL = 3
 SEQ_LEN = 256
 EPS = 1e-06
+
+
+def turn_shards_for(m, along_dim):
+    axis_total = axis_size("fs")
+    z2 = sorted(((i, (i + 1) % axis_total) for i in range(axis_total)))
+    x_next = m
+    pieces_in = [x_next]
+    for dev_j in range(1, axis_total):
+        x_next = ppermute(x_next, "fs", z2)
+        pieces_in.insert(0, x_next)
+    carry_out = jnp.concatenate(pieces_in, along_dim)
+    long_array = axis_index("fs") + 1
+    return jnp.roll(carry_out, long_array * m.shape[along_dim], along_dim)
 
 
 def matmul(operand, matrix):
@@ -86,7 +100,7 @@
         + mix_bias.astype(jnp.float32).T[None, :, :, None]
     )
     gated_rows = (act_u * spatial.reshape(row_count, mixed_in.shape[1])).astype(jnp.bfloat16)
-    whole_out = lax.all_gather(proj_out, "fs", axis=1, tiled=True)
+    whole_out = turn_shards_for(proj_out, 1)
     partial_value = matmul(gated_rows, whole_out)
     summed = lax.psum(partial_value.astype(jnp.bfloat16), "tp").astype(jnp.float32)
     stream_rows = (whole_tokens.astype(jnp.float32) + summed).astype(jnp.bfloat16)

time: 702 us -> 679 us (0.967)
  waiting for transfers between devices: 605 us -> 550 us
  local copies, waits for them, and re-layouts: 3.24 us -> 31.5 us
    ppermute x0 -> x15, waiting for transfers between devices: none -> 182 us  [turn_shards_for(): x_next = ppermute(x_next, 'fs', z2)]
    all_gather x1 -> x0, waiting for transfers between devices: 89.9 us -> none  [on_device(): whole_out = lax.all_gather(proj_out, 'fs', axis=1, tiled=True)]
    all_gather x1, waiting for transfers between devices: 77.3 us -> 0.01 us  [on_device(): lax.all_gather(proj_v, 'fs', axis=0, tiled=True)]
    all_gather x1, waiting for transfers between devices: 57.5 us -> 0.01 us  [on_device(): lax.all_gather(proj_u, 'fs', axis=0, tiled=True)]
    unnamed x15 -> x56, local copies, waits for them, and re-layouts: 0.29 us -> 27.8 us
    all_gather x1, waiting for transfers between devices: 8.57 us -> 0.01 us  [on_device(): lax.all_gather(tokens, 'tp', axis=1, tiled=True)]
  transfers between devices with their start and end apart: 9 -> 23, of which waited for: 9 -> 20; matrix products, arithmetic and copies ran while one was open for 7% -> 11% of each run, Pallas kernels for 0% -> 0%
where the time goes in v1:
time: 679 us; the launch traced here: 678 us
  waiting for transfers between devices  550 us (81%)
  matrix products  54.2 us (8%)
  local copies, waits for them, and re-layouts  31.5 us (5%)
  other arithmetic  18.6 us (3%)
  between operations  13.6 us (2%)
    ppermute x15, waiting for transfers between devices, turn_shards_for(): x_next = ppermute(x_next, 'fs', z2)  182 us
    all_gather x1, waiting for transfers between devices, on_device(): whole_down = lax.all_gather(proj_down, 'fs', axis=1, tiled=True)  129 us
    all_gather x1, waiting for transfers between devices, on_device(): lax.all_gather(ffn_gate, 'fs', axis=0, tiled=True)  112 us
    all_gather x1, waiting for transfers between devices, on_device(): lax.all_gather(ffn_value, 'fs', axis=0, tiled=True)  103 us
    dot_general x5, matrix products, matmul(): return jnp.dot(operand, matrix, preferred_element_type=jnp.float32)  52.4 us
    unnamed x56, local copies, waits for them, and re-layouts  27.8 us
  transfers between devices with their start and end apart: 23, of which 20 were waited for; matrix products, arithmetic and copies ran while one was open for 11% of the time, Pallas kernels for 0%

profile of v1, /device:TPU:0, one launch (start us, length us, event | category | flops | bytes accessed | tf_op | source)
XLA Modules:
  0.0 678.3 jit_solution(11970547701244843502)
XLA Ops:
  8.1 3.0 collective-permute-start
  11.1 10.5 %collective-permute-done = bf16[1024,128]{1,0:T(8,128)(2,1)S(1)} collective-permute-done((bf16[1024,128]{1,0:T(8,128)(2,1)}, bf16[1024,128]{1,0:T(8,128)(2,1)S(1)}, u32[]{:S(2)}, u32[]{:S(2)}) %collective-permute-start) | collective-permute-done | bytes 262176 | tf_op jit(solution)/shard_map/ppermute | solution.py:21
  21.6 11.1 %collective-permute-done.1 = bf16[1024,128]{1,0:T(8,128)(2,1)S(1)} collective-permute-done((bf16[1024,128]{1,0:T(8,128)(2,1)S(1)}, bf16[1024,128]{1,0:T(8,128)(2,1)S(1)}, u32[]{:S(2)}, u32[]{:S(2)}) %collective-permute-start.1) | collective-permute-done | bytes 262176 | tf_op jit(solution)/shard_map/ppermute | solution.py:21
  32.7 13.3 %collective-permute-done.2 = bf16[1024,128]{1,0:T(8,128)(2,1)S(1)} collective-permute-done((bf16[1024,128]{1,0:T(8,128)(2,1)S(1)}, bf16[1024,128]{1,0:T(8,128)(2,1)S(1)}, u32[]{:S(2)}, u32[]{:S(2)}) %collective-permute-start.2) | collective-permute-done | bytes 262176 | tf_op jit(solution)/shard_map/ppermute | solution.py:21
  46.0 10.0 %collective-permute-done.3 = bf16[1024,128]{1,0:T(8,128)(2,1)S(1)} collective-permute-done((bf16[1024,128]{1,0:T(8,128)(2,1)S(1)}, bf16[1024,128]{1,0:T(8,128)(2,1)S(1)}, u32[]{:S(2)}, u32[]{:S(2)}) %collective-permute-start.3) | collective-permute-done | bytes 262176 | tf_op jit(solution)/shard_map/ppermute | solution.py:21
  55.9 16.0 %collective-permute-done.4 = bf16[1024,128]{1,0:T(8,128)(2,1)S(1)} collective-permute-done((bf16[1024,128]{1,0:T(8,128)(2,1)S(1)}, bf16[1024,128]{1,0:T(8,128)(2,1)S(1)}, u32[]{:S(2)}, u32[]{:S(2)}) %collective-permute-start.4) | collective-permute-done | bytes 262176 | tf_op jit(solution)/shard_map/ppermute | solution.py:21
  71.9 12.1 %collective-permute-done.5 = bf16[1024,128]{1,0:T(8,128)(2,1)S(1)} collective-permute-done((bf16[1024,128]{1,0:T(8,128)(2,1)S(1)}, bf16[1024,128]{1,0:T(8,128)(2,1)S(1)}, u32[]{:S(2)}, u32[]{:S(2)}) %collective-permute-start.5) | collective-permute-done | bytes 262176 | tf_op jit(solution)/shard_map/ppermute | solution.py:21
  84.0 18.3 %collective-permute-done.6 = bf16[1024,128]{1,0:T(8,128)(2,1)S(1)} collective-permute-done((bf16[1024,128]{1,0:T(8,128)(2,1)S(1)}, bf16[1024,128]{1,0:T(8,128)(2,1)S(1)}, u32[]{:S(2)}, u32[]{:S(2)}) %collective-permute-start.6) | collective-permute-done | bytes 262176 | tf_op jit(solution)/shard_map/ppermute | solution.py:21
  102.3 15.4 %collective-permute-done.7 = bf16[1024,128]{1,0:T(8,128)(2,1)S(1)} collective-permute-done((bf16[1024,128]{1,0:T(8,128)(2,1)S(1)}, bf16[1024,128]{1,0:T(8,128)(2,1)S(1)}, u32[]{:S(2)}, u32[]{:S(2)}) %collective-permute-start.7) | collective-permute-done | bytes 262176 | tf_op jit(solution)/shard_map/ppermute | solution.py:21
  117.7 10.0 %collective-permute-done.8 = bf16[1024,128]{1,0:T(8,128)(2,1)S(1)} collective-permute-done((bf16[1024,128]{1,0:T(8,128)(2,1)S(1)}, bf16[1024,128]{1,0:T(8,128)(2,1)S(1)}, u32[]{:S(2)}, u32[]{:S(2)}) %collective-permute-start.8) | collective-permute-done | bytes 262176 | tf_op jit(solution)/shard_map/ppermute | solution.py:21
  127.6 10.0 %collective-permute-done.9 = bf16[1024,128]{1,0:T(8,128)(2,1)S(1)} collective-permute-done((bf16[1024,128]{1,0:T(8,128)(2,1)S(1)}, bf16[1024,128]{1,0:T(8,128)(2,1)S(1)}, u32[]{:S(2)}, u32[]{:S(2)}) %collective-permute-start.9) | collective-permute-done | bytes 262176 | tf_op jit(solution)/shard_map/ppermute | solution.py:21
  137.7 9.9 %collective-permute-done.10 = bf16[1024,128]{1,0:T(8,128)(2,1)S(1)} collective-permute-done((bf16[1024,128]{1,0:T(8,128)(2,1)S(1)}, bf16[1024,128]{1,0:T(8,128)(2,1)S(1)}, u32[]{:S(2)}, u32[]{:S(2)}) %collective-permute-start.10) | collective-permute-done | bytes 262176 | tf_op jit(solution)/shard_map/ppermute | solution.py:21
  147.6 17.0 %collective-permute-done.11 = bf16[1024,128]{1,0:T(8,128)(2,1)S(1)} collective-permute-done((bf16[1024,128]{1,0:T(8,128)(2,1)S(1)}, bf16[1024,128]{1,0:T(8,128)(2,1)S(1)}, u32[]{:S(2)}, u32[]{:S(2)}) %collective-permute-start.11) | collective-permute-done | bytes 262176 | tf_op jit(solution)/shard_map/ppermute | solution.py:21
  165.3 12.4 %collective-permute-done.12 = bf16[1024,128]{1,0:T(8,128)(2,1)S(1)} collective-permute-done((bf16[1024,128]{1,0:T(8,128)(2,1)S(1)}, bf16[1024,128]{1,0:T(8,128)(2,1)S(1)}, u32[]{:S(2)}, u32[]{:S(2)}) %collective-permute-start.12) | collective-permute-done | bytes 262176 | tf_op jit(solution)/shard_map/ppermute | solution.py:21
  177.7 2.0 all_gather.25
  181.2 8.0 %collective-permute-done.13 = bf16[1024,128]{1,0:T(8,128)(2,1)} collective-permute-done((bf16[1024,128]{1,0:T(8,128)(2,1)S(1)}, bf16[1024,128]{1,0:T(8,128)(2,1)}, u32[]{:S(2)}, u32[]{:S(2)}) %collective-permute-start.13) | collective-permute-done | bytes 262176 | tf_op jit(solution)/shard_map/ppermute | solution.py:21
  189.1 2.1 fusion.3
  191.2 8.3 %collective-permute-done.14 = bf16[1024,128]{1,0:T(8,128)(2,1)} collective-permute-done((bf16[1024,128]{1,0:T(8,128)(2,1)}, bf16[1024,128]{1,0:T(8,128)(2,1)}, u32[]{:S(2)}, u32[]{:S(2)}) %collective-permute-start.14) | collective-permute-done | bytes 262176 | tf_op jit(solution)/shard_map/ppermute | solution.py:21
  199.5 1.7 constant_dynamic-update-slice_fusion.31
  201.2 1.7 constant_dynamic-update-slice_fusion.30
  205.9 0.8 constant_dynamic-update-slice_fusion.25
  207.5 0.8 constant_dynamic-update-slice_fusion.23
  209.0 0.8 constant_dynamic-update-slice_fusion.21
  210.5 0.8 constant_dynamic-update-slice_fusion.19
  211.3 0.8 constant_dynamic-update-slice_fusion.18
  213.6 1.7 constant_dynamic-update-slice_fusion.15
  215.3 1.7 constant_dynamic-update-slice_fusion.14
  222.4 0.8 constant_dynamic-update-slice_fusion.6
  224.0 0.8 constant_dynamic-update-slice_fusion.4
  227.8 9.6 %fusion.117 = (f32[512]{0:T(512)S(1)}, f32[512]{0:T(512)S(1)}, f32[512,1024]{1,0:T(8,128)}) fusion(bf16[2048,1024]{1,0:T(8,128)(2,1)} %all-gather.11.cloned.1.call-done, bf16[512,2048]{1,0:T(8,128)(2,1)S(1)} %copy-done, f32[2048]{0:T(1024)S(1)} %convert_element_type.144, f32[512]{0:T(512)S(1)} %add_rsqrt_fusion.2), kind=kOutput, calls=%fused_computation.187 | convolution fusion | flops 2186804224 | bytes 8402944 | tf_op jit(solution)/shard_map/dot_general | solution.py:29
  237.4 2.6 all-reduce.2
  240.0 2.1 fusion.37
  242.4 1.8 bitcast_add_fusion
  244.2 2.9 copy.19
  247.1 14.5 %fusion.13 = bf16[512,2048]{1,0:T(8,128)(2,1)} fusion(bf16[1024,4096]{1,0:T(8,128)(2,1)} %constant_dynamic-update-slice_fusion, s32[]{:T(128)S(6)} %select_n.36, f32[64,8,8,128]{3,2,1,0:T(8,128)} %bitcast.50, bf16[2048,1024]{1,0:T(8,128)(2,1)} %all-gather.9.cloned.1.call-done, bf16[512,2048]{1,0:T(8,128)(2,1)S(1)} %copy-done, ...), kind=kOutput, calls=%fused_computation.25 | convolution fusion | flops 4334813184 | bytes 14690308 | tf_op jit(solution)/shard_map/dot_general | solution.py:29
  263.6 2.1 all_gather.28
  265.7 13.3 %all-reduce.5.cloned.1.call-done = bf16[512,2048]{1,0:T(8,128)(2,1)} async-done(((bf16[512,2048]{1,0:T(8,128)(2,1)}), bf16[512,2048]{1,0:T(8,128)(2,1)}) %all-reduce.5.cloned.1.call-update) | async-done | bytes 2097168 | tf_op jit(solution)/shard_map/psum | solution.py:105
  279.0 3.9 fusion
  282.9 112.2 %all-gather.13.cloned.1.call-done = bf16[2048,2048]{1,0:T(8,128)(2,1)} async-done(((bf16[128,2048]{1,0:T(8,128)(2,1)}), bf16[2048,2048]{1,0:T(8,128)(2,1)}) %all-gather.13.cloned.1.call-update) | async-done | bytes 8388624 | tf_op jit(solution)/shard_map/all_gather | solution.py:110
  395.1 10.1 %convolution_convert_fusion.2 = bf16[512,2048]{1,0:T(8,128)(2,1)} fusion(bf16[2048,2048]{1,0:T(8,128)(2,1)} %all-gather.13.cloned.1.call-done, bf16[512,2048]{1,0:T(8,128)(2,1)} %get-tuple-element.10, f32[2048]{0:T(1024)S(1)} %convert_element_type.155, f32[512]{0:T(512)S(1)} %add_rsqrt_fusion), kind=kOutput, calls=%fused_computation.28 | convolution fusion | flops 4300210176 | bytes 12593152 | tf_op jit(solution)/shard_map/dot_general | solution.py:29
  405.2 103.1 %all-gather.15.cloned.1.call-done = bf16[2048,2048]{1,0:T(8,128)(2,1)} async-done(((bf16[128,2048]{1,0:T(8,128)(2,1)}), bf16[2048,2048]{1,0:T(8,128)(2,1)}) %all-gather.15.cloned.1.call-update) | async-done | bytes 8388624 | tf_op jit(solution)/shard_map/all_gather | solution.py:111
  508.3 8.4 %convolution_convert_fusion.1 = bf16[512,2048]{1,0:T(8,128)(2,1)S(1)} fusion(bf16[2048,2048]{1,0:T(8,128)(2,1)} %all-gather.15.cloned.1.call-done, bf16[512,2048]{1,0:T(8,128)(2,1)S(1)} %copy-done.1, f32[2048]{0:T(1024)S(1)} %convert_element_type.155, f32[512]{0:T(512)S(1)} %add_rsqrt_fusion), kind=kOutput, calls=%fused_computation.27 | convolution fusion | flops 4300210176 | bytes 12593152 | tf_op jit(solution)/shard_map/dot_general | solution.py:29
  516.7 3.0 multiply_add_fusion
  519.7 2.6 fusion.7
  522.3 128.7 %all-gather.17.cloned.1.call-done = bf16[2048,2048]{1,0:T(8,128)(2,1)} async-done(((bf16[2048,128]{1,0:T(8,128)(2,1)}), bf16[2048,2048]{1,0:T(8,128)(2,1)}) %all-gather.17.cloned.1.call-update) | async-done | bytes 8388624 | tf_op jit(solution)/shard_map/all_gather | solution.py:118
  651.0 9.9 %convolution_convert_fusion = bf16[512,2048]{1,0:T(8,128)(2,1)} fusion(bf16[512,2048]{1,0:T(8,128)(2,1)} %fusion.7, bf16[2048,2048]{1,0:T(8,128)(2,1)} %all-gather.17.cloned.1.call-done), kind=kOutput, calls=%fused_computation.26 | convolution fusion | flops 4296015872 | bytes 12582912 | tf_op jit(solution)/shard_map/dot_general | solution.py:29
  660.9 8.0 %reduce-scatter.2.cloned.1.call-done = bf16[512,1024]{1,0:T(8,128)(2,1)} async-done(((bf16[512,2048]{1,0:T(8,128)(2,1)}), bf16[512,1024]{1,0:T(8,128)(2,1)}) %reduce-scatter.2.cloned.1.call-update) | async-done | bytes 1048592 | tf_op jit(solution)/shard_map/reduce_scatter | solution.py:122
  668.9 2.6 add_convert_fusion
  (91 shorter events, 21.9 us)
Async XLA Ops:
  6.5 182.6 %all-gather.7.cloned.1.call-start = ((), (), s32[]{:S(2)}) async-start(), calls=%async_computation.1 | async-start | bytes 3145728 | tf_op jit(solution)/shard_map/all_gather | solution.py:69
  7.3 220.5 %all-gather.11.cloned.1.call-start = ((), (), s32[]{:S(2)}) async-start(), calls=%async_computation.3 | async-start | bytes 4456448 | tf_op jit(solution)/shard_map/all_gather | solution.py:77
  8.0 239.1 %all-gather.9.cloned.1.call-start = ((), (), s32[]{:S(2)}) async-start(), calls=%async_computation.2 | async-start | bytes 4456448 | tf_op jit(solution)/shard_map/all_gather | solution.py:76
  8.1 13.5 %collective-permute-start = (bf16[1024,128]{1,0:T(8,128)(2,1)}, bf16[1024,128]{1,0:T(8,128)(2,1)S(1)}, u32[]{:S(2)}, u32[]{:S(2)}) collective-permute-start(bf16[1024,128]{1,0:T(8,128)(2,1)} %param.23), channel_id=1, source_target_pairs={{0,2},{2,4},{4,6},{6,8},{8,10},{10,12},{12,14},{14,16},{16,18},{18... | collective-permute-start | bytes 786440 | tf_op jit(solution)/shard_map/ppermute | solution.py:21
  21.6 11.1 %collective-permute-start.1 = (bf16[1024,128]{1,0:T(8,128)(2,1)S(1)}, bf16[1024,128]{1,0:T(8,128)(2,1)S(1)}, u32[]{:S(2)}, u32[]{:S(2)}) collective-permute-start(bf16[1024,128]{1,0:T(8,128)(2,1)S(1)} %collective-permute-done), channel_id=1, source_target_pairs={{0,2},{2,4},{4,6},{6,8},{8,10},{10,12},{12,14},{14,16},{16,18},{18... | collective-permute-start | bytes 786440 | tf_op jit(solution)/shard_map/ppermute | solution.py:21
  32.6 13.3 %collective-permute-start.2 = (bf16[1024,128]{1,0:T(8,128)(2,1)S(1)}, bf16[1024,128]{1,0:T(8,128)(2,1)S(1)}, u32[]{:S(2)}, u32[]{:S(2)}) collective-permute-start(bf16[1024,128]{1,0:T(8,128)(2,1)S(1)} %collective-permute-done.1), channel_id=1, source_target_pairs={{0,2},{2,4},{4,6},{6,8},{8,10},{10,12},{12,14},{14,16},{16,18},{18... | collective-permute-start | bytes 786440 | tf_op jit(solution)/shard_map/ppermute | solution.py:21
  46.0 10.0 %collective-permute-start.3 = (bf16[1024,128]{1,0:T(8,128)(2,1)S(1)}, bf16[1024,128]{1,0:T(8,128)(2,1)S(1)}, u32[]{:S(2)}, u32[]{:S(2)}) collective-permute-start(bf16[1024,128]{1,0:T(8,128)(2,1)S(1)} %collective-permute-done.2), channel_id=1, source_target_pairs={{0,2},{2,4},{4,6},{6,8},{8,10},{10,12},{12,14},{14,16},{16,18},{18... | collective-permute-start | bytes 786440 | tf_op jit(solution)/shard_map/ppermute | solution.py:21
  55.9 16.0 %collective-permute-start.4 = (bf16[1024,128]{1,0:T(8,128)(2,1)S(1)}, bf16[1024,128]{1,0:T(8,128)(2,1)S(1)}, u32[]{:S(2)}, u32[]{:S(2)}) collective-permute-start(bf16[1024,128]{1,0:T(8,128)(2,1)S(1)} %collective-permute-done.3), channel_id=1, source_target_pairs={{0,2},{2,4},{4,6},{6,8},{8,10},{10,12},{12,14},{14,16},{16,18},{18... | collective-permute-start | bytes 786440 | tf_op jit(solution)/shard_map/ppermute | solution.py:21
  71.9 12.1 %collective-permute-start.5 = (bf16[1024,128]{1,0:T(8,128)(2,1)S(1)}, bf16[1024,128]{1,0:T(8,128)(2,1)S(1)}, u32[]{:S(2)}, u32[]{:S(2)}) collective-permute-start(bf16[1024,128]{1,0:T(8,128)(2,1)S(1)} %collective-permute-done.4), channel_id=1, source_target_pairs={{0,2},{2,4},{4,6},{6,8},{8,10},{10,12},{12,14},{14,16},{16,18},{18... | collective-permute-start | bytes 786440 | tf_op jit(solution)/shard_map/ppermute | solution.py:21
  84.0 124.3 %copy-start.4 = (bf16[1024,128]{1,0:T(8,128)(2,1)}, bf16[1024,128]{1,0:T(8,128)(2,1)S(1)}, u32[]{:S(2)}) copy-start(bf16[1024,128]{1,0:T(8,128)(2,1)S(1)} %collective-permute-done.5) | copy-start | bytes 786436
  84.0 18.3 %collective-permute-start.6 = (bf16[1024,128]{1,0:T(8,128)(2,1)S(1)}, bf16[1024,128]{1,0:T(8,128)(2,1)S(1)}, u32[]{:S(2)}, u32[]{:S(2)}) collective-permute-start(bf16[1024,128]{1,0:T(8,128)(2,1)S(1)} %collective-permute-done.5), channel_id=1, source_target_pairs={{0,2},{2,4},{4,6},{6,8},{8,10},{10,12},{12,14},{14,16},{16,18},{18... | collective-permute-start | bytes 786440 | tf_op jit(solution)/shard_map/ppermute | solution.py:21
  102.3 105.2 %copy-start.6 = (bf16[1024,128]{1,0:T(8,128)(2,1)}, bf16[1024,128]{1,0:T(8,128)(2,1)S(1)}, u32[]{:S(2)}) copy-start(bf16[1024,128]{1,0:T(8,128)(2,1)S(1)} %collective-permute-done.6) | copy-start | bytes 786436
  102.3 15.4 %collective-permute-start.7 = (bf16[1024,128]{1,0:T(8,128)(2,1)S(1)}, bf16[1024,128]{1,0:T(8,128)(2,1)S(1)}, u32[]{:S(2)}, u32[]{:S(2)}) collective-permute-start(bf16[1024,128]{1,0:T(8,128)(2,1)S(1)} %collective-permute-done.6), channel_id=1, source_target_pairs={{0,2},{2,4},{4,6},{6,8},{8,10},{10,12},{12,14},{14,16},{16,18},{18... | collective-permute-start | bytes 786440 | tf_op jit(solution)/shard_map/ppermute | solution.py:21
  117.7 10.0 %collective-permute-start.8 = (bf16[1024,128]{1,0:T(8,128)(2,1)S(1)}, bf16[1024,128]{1,0:T(8,128)(2,1)S(1)}, u32[]{:S(2)}, u32[]{:S(2)}) collective-permute-start(bf16[1024,128]{1,0:T(8,128)(2,1)S(1)} %collective-permute-done.7), channel_id=1, source_target_pairs={{0,2},{2,4},{4,6},{6,8},{8,10},{10,12},{12,14},{14,16},{16,18},{18... | collective-permute-start | bytes 786440 | tf_op jit(solution)/shard_map/ppermute | solution.py:21
  127.6 10.0 %collective-permute-start.9 = (bf16[1024,128]{1,0:T(8,128)(2,1)S(1)}, bf16[1024,128]{1,0:T(8,128)(2,1)S(1)}, u32[]{:S(2)}, u32[]{:S(2)}) collective-permute-start(bf16[1024,128]{1,0:T(8,128)(2,1)S(1)} %collective-permute-done.8), channel_id=1, source_target_pairs={{0,2},{2,4},{4,6},{6,8},{8,10},{10,12},{12,14},{14,16},{16,18},{18... | collective-permute-start | bytes 786440 | tf_op jit(solution)/shard_map/ppermute | solution.py:21
  137.6 10.0 %collective-permute-start.10 = (bf16[1024,128]{1,0:T(8,128)(2,1)S(1)}, bf16[1024,128]{1,0:T(8,128)(2,1)S(1)}, u32[]{:S(2)}, u32[]{:S(2)}) collective-permute-start(bf16[1024,128]{1,0:T(8,128)(2,1)S(1)} %collective-permute-done.9), channel_id=1, source_target_pairs={{0,2},{2,4},{4,6},{6,8},{8,10},{10,12},{12,14},{14,16},{16,18},{18... | collective-permute-start | bytes 786440 | tf_op jit(solution)/shard_map/ppermute | solution.py:21
  137.6 141.4 %all-reduce.5.cloned.1.call-start = ((), (), s32[]{:S(2)}) async-start(), calls=%async_computation.4 | async-start | bytes 4194304 | tf_op jit(solution)/shard_map/psum | solution.py:105
  147.6 17.0 %collective-permute-start.11 = (bf16[1024,128]{1,0:T(8,128)(2,1)S(1)}, bf16[1024,128]{1,0:T(8,128)(2,1)S(1)}, u32[]{:S(2)}, u32[]{:S(2)}) collective-permute-start(bf16[1024,128]{1,0:T(8,128)(2,1)S(1)} %collective-permute-done.10), channel_id=1, source_target_pairs={{0,2},{2,4},{4,6},{6,8},{8,10},{10,12},{12,14},{14,16},{16,18},{18... | collective-permute-start | bytes 786440 | tf_op jit(solution)/shard_map/ppermute | solution.py:21
  164.6 13.1 %collective-permute-start.12 = (bf16[1024,128]{1,0:T(8,128)(2,1)S(1)}, bf16[1024,128]{1,0:T(8,128)(2,1)S(1)}, u32[]{:S(2)}, u32[]{:S(2)}) collective-permute-start(bf16[1024,128]{1,0:T(8,128)(2,1)S(1)} %collective-permute-done.11), channel_id=1, source_target_pairs={{0,2},{2,4},{4,6},{6,8},{8,10},{10,12},{12,14},{14,16},{16,18},{18... | collective-permute-start | bytes 786440 | tf_op jit(solution)/shard_map/ppermute | solution.py:21
  177.7 11.4 %collective-permute-start.13 = (bf16[1024,128]{1,0:T(8,128)(2,1)S(1)}, bf16[1024,128]{1,0:T(8,128)(2,1)}, u32[]{:S(2)}, u32[]{:S(2)}) collective-permute-start(bf16[1024,128]{1,0:T(8,128)(2,1)S(1)} %collective-permute-done.12), channel_id=1, source_target_pairs={{0,2},{2,4},{4,6},{6,8},{8,10},{10,12},{12,14},{14,16},{16,18},{18... | collective-permute-start | bytes 786440 | tf_op jit(solution)/shard_map/ppermute | solution.py:21
  189.1 10.3 %collective-permute-start.14 = (bf16[1024,128]{1,0:T(8,128)(2,1)}, bf16[1024,128]{1,0:T(8,128)(2,1)}, u32[]{:S(2)}, u32[]{:S(2)}) collective-permute-start(bf16[1024,128]{1,0:T(8,128)(2,1)} %collective-permute-done.13), channel_id=1, source_target_pairs={{0,2},{2,4},{4,6},{6,8},{8,10},{10,12},{12,14},{14,16},{16,18},{18... | collective-permute-start | bytes 786440 | tf_op jit(solution)/shard_map/ppermute | solution.py:21
  206.7 6.2 copy-start.3
  213.6 8.1 %copy-start.7 = (bf16[1024,128]{1,0:T(8,128)(2,1)S(1)}, bf16[1024,128]{1,0:T(8,128)(2,1)}, u32[]{:S(2)}) copy-start(bf16[1024,128]{1,0:T(8,128)(2,1)} %copy-done.6) | copy-start | bytes 786436
  215.3 7.1 %copy-start.5 = (bf16[1024,128]{1,0:T(8,128)(2,1)S(1)}, bf16[1024,128]{1,0:T(8,128)(2,1)}, u32[]{:S(2)}) copy-start(bf16[1024,128]{1,0:T(8,128)(2,1)} %copy-done.4) | copy-start | bytes 786436
  221.7 6.1 copy-start
  240.0 2.4 copy-start.8
  261.6 2.0 copy-start.11
  261.6 4.1 copy-start.9
  261.6 4.1 copy-start.10
  261.6 133.5 %all-gather.13.cloned.1.call-start = ((), (), s32[]{:S(2)}) async-start(), calls=%async_computation.5 | async-start | bytes 8912896 | tf_op jit(solution)/shard_map/all_gather | solution.py:110
  262.2 246.0 %all-gather.15.cloned.1.call-start = ((), (), s32[]{:S(2)}) async-start(), calls=%async_computation.6 | async-start | bytes 8912896 | tf_op jit(solution)/shard_map/all_gather | solution.py:111
  262.8 388.2 %all-gather.17.cloned.1.call-start = ((), (), s32[]{:S(2)}) async-start(), calls=%async_computation.7 | async-start | bytes 8912896 | tf_op jit(solution)/shard_map/all_gather | solution.py:118
  263.5 405.3 %reduce-scatter.2.cloned.1.call-start = ((), (), s32[]{:S(2)}) async-start(), calls=%async_computation.8 | async-start | bytes 3145728 | tf_op jit(solution)/shard_map/reduce_scatter | solution.py:122
  395.1 113.1 %copy-start.1 = (bf16[512,2048]{1,0:T(8,128)(2,1)S(1)}, bf16[512,2048]{1,0:T(8,128)(2,1)}, u32[]{:S(2)}) copy-start(bf16[512,2048]{1,0:T(8,128)(2,1)} %get-tuple-element.10) | copy-start | bytes 6291460
  508.3 8.4 %copy-start.2 = (bf16[512,2048]{1,0:T(8,128)(2,1)S(1)}, bf16[512,2048]{1,0:T(8,128)(2,1)}, u32[]{:S(2)}) copy-start(bf16[512,2048]{1,0:T(8,128)(2,1)} %convolution_convert_fusion.2) | copy-start | bytes 6291460
Sparse Core Ops, SparseCore 0:
  8.9 13.2 all-gather.6
  25.0 93.1 all-gather.10
  137.7 86.9 all-gather.8
  261.7 17.1 all-reduce.4
  281.6 113.4 all-gather.12
  397.8 110.4 all-gather.14
  511.0 139.9 all-gather.16
  661.0 7.7 reduce-scatter.1
